TPU v7x, 32 devices: a whole 2x2x4 slice. The times are simulated.
32 devices in a mesh: sp: 16 (over z, y, core), tp: 2 (over x).
Axes of the slice: x: 2, y: 2, z: 4, core: 2. Of those that a mesh axis runs over, the one named last changes fastest.
Arguments:
- residual: bfloat16 [2048, 2048], P(('sp', 'tp')), may hold values from -6 to 6
- forget_forward: bfloat16 [2048, 1024], P('sp', 'tp'), may hold values from -5.5 to 5.5
- forget_backward: bfloat16 [2048, 1024], P('sp', 'tp'), may hold values from -5.5 to 5.5
- value_written: bfloat16 [2048, 1024], P('sp', 'tp'), may hold values from -6 to 6
- query_logits: bfloat16 [2048, 1024], P('sp', 'tp'), may hold values from -6 to 6
- output_gate_logits: bfloat16 [2048, 1024], P('sp', 'tp'), may hold values from -6 to 6
- forget_minimum: float32 [2, 1024], P(None, 'tp'), may hold values from 0.88 to 1
- extra_log_rate: float32 [2, 2048, 8], P(None, 'sp', 'tp'), may hold values from -0.7 to 0
- head_norm_scale: float32 [128], replicated, may hold values from 0.1 to 1.9
- output_matrix: bfloat16 [1024, 2048], P(None, 'sp'), may hold values from -0.1875 to 0.1875
- prenorm_scale: float32 [2048], replicated, may hold values from 0.1 to 1.9
- gate_up_matrix: bfloat16 [2048, 5632], P('sp', 'tp'), may hold values from -0.125 to 0.125
- value_up_matrix: bfloat16 [2048, 5632], P('sp', 'tp'), may hold values from -0.125 to 0.125
- gate_taps: float32 [3, 5632], P(None, 'tp'), may hold values from -3.5 to 3.5
- value_taps: float32 [3, 5632], P(None, 'tp'), may hold values from -3.5 to 3.5
- down_matrix: bfloat16 [5632, 2048], P('tp', 'sp'), may hold values from -0.078125 to 0.078125
Outputs:
- layer_out: bfloat16 [2048, 2048], P(('sp', 'tp'))
All inputs are finite; a program needn't handle non-finite values.
Results may differ from a plain program's by a relative error of at most 0.012.
Values may be sent and summed in bfloat16 or wider, within the bound.
A program may use at most 128 MiB of HBM per device.

v0:
```python
import jax
import jax.numpy as jnp
from jax import lax
from jax.sharding import PartitionSpec as P

HEAD_WIDTH = 128
BLOCK = 64


EPSILON = 1e-06


def carried_in(array, axis, combine, identity, reverse):
    size, position = (lax.axis_size(axis), lax.axis_index(axis))
    everything = jax.tree.map(
        lambda part, kind: lax.all_gather(part.astype(kind), axis),
        array,
        (jnp.bfloat16, jnp.bfloat16),
    )
    start = jax.tree.map(
        lambda part, zero: jnp.broadcast_to(jnp.asarray(zero, part.dtype), part.shape),
        array,
        identity,
    )

    def hop(k, before):
        at = size - 1 - k if reverse else k
        reached = at > position if reverse else at < position
        new = combine(
            before, jax.tree.map(lambda part, own: part[at].astype(own.dtype), everything, array)
        )
        return jax.tree.map(lambda a, b: jnp.where(reached, a, b), new, before)

    return lax.fori_loop(0, size, hop, start)


def extended(array, sides, width):
    for axis, dim in sides:
        size, length = (lax.axis_size(axis), array.shape[dim])
        up = [(i, (i + 1) % size) for i in range(size - 1)]
        down = [(j, i) for i, j in up]
        last = lax.slice_in_dim(array, length - width, length, axis=dim)
        initial = lax.slice_in_dim(array, 0, width, axis=dim)
        before = lax.ppermute(last, axis, up)
        after = lax.ppermute(initial, axis, down)
        array = jnp.concatenate([before, array, after], axis=dim)
    return array


def rms_scale(array):
    return array * lax.rsqrt(jnp.mean(array * array, axis=-1, keepdims=True) + EPSILON)


def forget_factors(forget_logits, forget_floor, extra_decay):
    unbounded_gate = forget_logits.astype(jnp.float32)
    log_forget_gate = jnp.log(
        forget_floor + (1.0 - forget_floor) * jax.nn.sigmoid(unbounded_gate)
    ) + jnp.repeat(extra_decay, HEAD_WIDTH, axis=1)
    key_in = (1.0 - forget_floor) * jax.nn.sigmoid(-unbounded_gate)
    shape = (unbounded_gate.shape[0], unbounded_gate.shape[1] // HEAD_WIDTH, HEAD_WIDTH)
    return (log_forget_gate.reshape(shape), key_in.reshape(shape))


def block_scan(log_forget_gate, key_in, values, queries):
    length, heads, depth = log_forget_gate.shape
    width = values.shape[2]
    blocks = length // BLOCK
    highest = lax.Precision.HIGHEST
    lower = jnp.tril(jnp.ones((BLOCK, BLOCK), dtype=bool))[:, :, None, None]

    def split(array):
        return array.reshape(blocks, BLOCK, heads, array.shape[2])

    def advance(carry, pieces):
        state, carried = carry
        log_part, key_part, value_part, query_part = pieces
        running = jnp.cumsum(log_part, axis=0)
        block_total = running[-1]
        query_carry = query_part * jnp.exp(carried[None] + running)
        from_state = jnp.einsum(
            "chd,hde->che", query_part * jnp.exp(running), state, precision=highest
        )
        gaps = jnp.where(lower, running[:, None] - running[None, :], -1e30)
        scores = jnp.einsum(
            "ihd,jhd,ijhd->hij", query_part, key_part, jnp.exp(gaps), precision=highest
        )
        inside = jnp.einsum("hij,jhe->ihe", scores, value_part, precision=highest)
        fresh = jnp.einsum(
            "chd,che->hde",
            key_part * jnp.exp(block_total[None] - running),
            value_part,
            precision=highest,
        )
        state = jnp.exp(block_total)[:, :, None] * state + fresh
        return ((state, carried + block_total), (from_state + inside, query_carry))

    start = (jnp.zeros((heads, depth, width), jnp.float32), jnp.zeros((heads, depth), jnp.float32))
    (state, carried), (outputs, query_carry) = lax.scan(
        advance, start, (split(log_forget_gate), split(key_in), split(values), split(queries))
    )
    return (
        state,
        carried,
        outputs.reshape(length, heads, width),
        query_carry.reshape(length, heads, depth),
    )


def link_states(earlier, later):
    return (earlier[0] + later[0], jnp.exp(later[0])[:, :, None] * earlier[1] + later[1])


def on_device(
    residual,
    forget_forward,
    forget_backward,
    value_written,
    query_logits,
    output_gate_logits,
    forget_minimum,
    extra_log_rate,
    head_norm_scale,
    output_matrix,
    prenorm_scale,
    gate_up_matrix,
    value_up_matrix,
    gate_taps,
    value_taps,
    down_matrix,
):
    highest = lax.Precision.HIGHEST
    length = value_written.shape[0]
    shape = (length, value_written.shape[1] // HEAD_WIDTH, HEAD_WIDTH)
    gate_full, value_full, down_full, out_full = (
        lax.all_gather(gate_up_matrix, "sp", axis=0, tiled=True),
        lax.all_gather(value_up_matrix, "sp", axis=0, tiled=True),
        lax.all_gather(down_matrix, "sp", axis=1, tiled=True),
        lax.all_gather(output_matrix, "sp", axis=1, tiled=True),
    )
    values = value_written.astype(jnp.float32).reshape(shape)
    queries = jax.nn.silu(query_logits.astype(jnp.float32)).reshape(shape)
    log_decay_forward, key_forward = forget_factors(
        forget_forward, forget_minimum[0], extra_log_rate[0]
    )
    state, carried, forward, carry_fwd = block_scan(log_decay_forward, key_forward, values, queries)
    empty = (jnp.zeros_like(carried), jnp.zeros_like(state))
    entering = carried_in((carried, state), "sp", link_states, empty, False)
    forward = forward + jnp.einsum("thd,hde->the", carry_fwd, entering[1], precision=highest)
    log_decay_backward, key_backward = forget_factors(
        forget_backward, forget_minimum[1], extra_log_rate[1]
    )
    state, carried, backward, carry_bwd = block_scan(
        log_decay_backward[::-1], key_backward[::-1], values[::-1], queries[::-1]
    )
    entering = carried_in((carried, state), "sp", link_states, empty, True)
    backward = (backward + jnp.einsum("thd,hde->the", carry_bwd, entering[1], precision=highest))[
        ::-1
    ]
    gated = (
        rms_scale(forward + backward)
        * head_norm_scale
        * jax.nn.silu(output_gate_logits.astype(jnp.float32)).reshape(shape)
    )
    mixed_in = gated.reshape(length, shape[1] * HEAD_WIDTH).astype(jnp.bfloat16)
    token_rows = lax.all_to_all(mixed_in, "tp", split_axis=0, concat_axis=1, tiled=True)
    mixed = jnp.dot(token_rows, out_full, preferred_element_type=jnp.float32)
    own_after = residual.astype(jnp.float32) + mixed
    normed = (rms_scale(own_after) * prenorm_scale).astype(jnp.bfloat16)
    normed_all = lax.all_gather(normed, "tp", axis=0, tiled=True)
    gate_up = jnp.dot(normed_all, gate_full, preferred_element_type=jnp.float32)
    value_up = jnp.dot(normed_all, value_full, preferred_element_type=jnp.float32)
    upward = jnp.concatenate([gate_up.astype(jnp.bfloat16), value_up.astype(jnp.bfloat16)], axis=1)
    padded = extended(upward, (("sp", 0),), 1)
    kernel = jnp.concatenate([gate_taps, value_taps], axis=1)
    convolved = (
        padded[:length] * kernel[0] + padded[1 : length + 1] * kernel[1] + padded[2:] * kernel[2]
    )
    hidden_width = gate_up_matrix.shape[1]
    hidden = (jax.nn.silu(convolved[:, :hidden_width]) * convolved[:, hidden_width:]).astype(
        jnp.bfloat16
    )
    terms = jnp.dot(hidden, down_full, preferred_element_type=jnp.float32)
    down_sum = lax.psum_scatter(
        terms.astype(jnp.bfloat16), "tp", scatter_dimension=0, tiled=True
    ).astype(jnp.float32)
    return (own_after + down_sum).astype(jnp.bfloat16)


def solution(mesh):
    return jax.shard_map(
        on_device,
        mesh=mesh,
        in_specs=(
            P(("sp", "tp"), None),
            P("sp", "tp"),
            P("sp", "tp"),
            P("sp", "tp"),
            P("sp", "tp"),
            P("sp", "tp"),
            P(None, "tp"),
            P(None, "sp", "tp"),
            P(),
            P(None, "sp"),
            P(),
            P("sp", "tp"),
            P("sp", "tp"),
            P(None, "tp"),
            P(None, "tp"),
            P("tp", "sp"),
        ),
        out_specs=P(("sp", "tp"), None),
        check_vma=False,
    )
```

profile of v0, /device:TPU:0, one launch (start us, length us, event | category | flops | bytes accessed | tf_op | source)
XLA Modules:
  0.0 496.8 jit_solution(2763869349589642076)
XLA Ops:
  8.3 1.1 fusion.86
  10.7 29.9 %while.66 = (s32[]{:T(128)}, f32[4,128,128]{2,1,0:T(8,128)S(1)}, f32[4,128]{1,0:T(4,128)S(1)}, f32[2,64,4,128]{3,1,0,2:T(8,128)S(1)}, f32[2,64,4,128]{3,2,1,0:T(...) while((s32[]{:T(128)}, f32[4,128,128]{2,1,0:T(8,128)S(1)}, ...), condition=%wide.region_7.8_spmd.clone, body=%wide.region_5.7_spmd.clone.sunk | while | flops 138826752 | bytes 21328020 | solution.py:98
  11.0 5.9 %exponential_bitcast_fusion.10 = f32[4,64,64,128]{3,0,2,1:T(4,128)S(1)} fusion(f32[64,4,128]{2,1,0:T(4,128)S(1)} %fusion.156, pred[64,64]{1,0:T(8,128)(4,1)S(1)} %fusion.158), kind=kLoop, calls=%fused_computation.49.clone.1 | loop fusion | flops 4194304 | bytes 8523776 | tf_op jit(solution)/shard_map/while
  16.9 7.3 %fusion.160 = f32[4,64,64]{1,2,0:T(8,128)S(1)} fusion(f32[4,64,64,128]{3,0,2,1:T(4,128)S(1)} %exponential_bitcast_fusion.10, f32[4,128,64]{1,2,0:T(8,128)S(1)} %copy.239, f32[4,128,64]{1,2,0:T(8,128)S(1)} %copy.240), kind=kLoop, calls=%fused_computation.48.clone.1 | loop fusion | flops 6275072 | bytes 8716288 | tf_op jit(solution)/shard_map/while/body/eval_jaxpr/ihd,jhd,ijhd->hij/dot_general | solution.py:84
  25.9 5.9 %exponential_bitcast_fusion.10 = f32[4,64,64,128]{3,0,2,1:T(4,128)S(1)} fusion(f32[64,4,128]{2,1,0:T(4,128)S(1)} %fusion.156, pred[64,64]{1,0:T(8,128)(4,1)S(1)} %fusion.158), kind=kLoop, calls=%fused_computation.49.clone.1 | loop fusion | flops 4194304 | bytes 8523776 | tf_op jit(solution)/shard_map/while
  31.8 7.3 %fusion.160 = f32[4,64,64]{1,2,0:T(8,128)S(1)} fusion(f32[4,64,64,128]{3,0,2,1:T(4,128)S(1)} %exponential_bitcast_fusion.10, f32[4,128,64]{1,2,0:T(8,128)S(1)} %copy.239, f32[4,128,64]{1,2,0:T(8,128)S(1)} %copy.240), kind=kLoop, calls=%fused_computation.48.clone.1 | loop fusion | flops 6275072 | bytes 8716288 | tf_op jit(solution)/shard_map/while/body/eval_jaxpr/ihd,jhd,ijhd->hij/dot_general | solution.py:84
  43.0 29.9 %while.64 = (s32[]{:T(128)}, f32[4,128,128]{2,1,0:T(8,128)S(1)}, f32[4,128]{1,0:T(4,128)S(1)}, f32[2,64,4,128]{3,1,0,2:T(8,128)S(1)}, f32[2,64,4,128]{3,2,1,0:T(...) while((s32[]{:T(128)}, f32[4,128,128]{2,1,0:T(8,128)S(1)}, ...), condition=%wide.region_2.3_spmd.clone, body=%wide.region_0.2_spmd.clone.sunk | while | flops 138826752 | bytes 21328020 | solution.py:98
  43.2 5.9 %exponential_bitcast_fusion.8 = f32[4,64,64,128]{3,0,2,1:T(4,128)S(1)} fusion(f32[64,4,128]{2,1,0:T(4,128)S(1)} %fusion.142, pred[64,64]{1,0:T(8,128)(4,1)S(1)} %fusion.144), kind=kLoop, calls=%fused_computation.10.clone.1 | loop fusion | flops 4194304 | bytes 8523776 | tf_op jit(solution)/shard_map/while
  49.1 7.3 %fusion.146 = f32[4,64,64]{1,2,0:T(8,128)S(1)} fusion(f32[4,64,64,128]{3,0,2,1:T(4,128)S(1)} %exponential_bitcast_fusion.8, f32[4,128,64]{1,2,0:T(8,128)S(1)} %copy.234, f32[4,128,64]{1,2,0:T(8,128)S(1)} %copy.235), kind=kLoop, calls=%fused_computation.9.clone.1 | loop fusion | flops 6275072 | bytes 8716288 | tf_op jit(solution)/shard_map/while/body/eval_jaxpr/ihd,jhd,ijhd->hij/dot_general | solution.py:84
  58.2 5.9 %exponential_bitcast_fusion.8 = f32[4,64,64,128]{3,0,2,1:T(4,128)S(1)} fusion(f32[64,4,128]{2,1,0:T(4,128)S(1)} %fusion.142, pred[64,64]{1,0:T(8,128)(4,1)S(1)} %fusion.144), kind=kLoop, calls=%fused_computation.10.clone.1 | loop fusion | flops 4194304 | bytes 8523776 | tf_op jit(solution)/shard_map/while
  64.1 7.3 %fusion.146 = f32[4,64,64]{1,2,0:T(8,128)S(1)} fusion(f32[4,64,64,128]{3,0,2,1:T(4,128)S(1)} %exponential_bitcast_fusion.8, f32[4,128,64]{1,2,0:T(8,128)S(1)} %copy.234, f32[4,128,64]{1,2,0:T(8,128)S(1)} %copy.235), kind=kLoop, calls=%fused_computation.9.clone.1 | loop fusion | flops 6275072 | bytes 8716288 | tf_op jit(solution)/shard_map/while/body/eval_jaxpr/ihd,jhd,ijhd->hij/dot_general | solution.py:84
  76.6 23.2 %all-gather.5 = bf16[16,4,128]{2,1,0:T(4,128)(2,1)S(1)} all-gather(bf16[1,4,128]{2,1,0:T(4,128)(2,1)S(1)} %convert_bitcast_fusion), channel_id=4, replica_groups=mesh['sp'=16,'tp'=2] {'sp'}, dimensions={0}, use_global_device_ids=true | all-gather | bytes 17408 | tf_op jit(solution)/shard_map/all_gather | solution.py:16
  99.8 17.7 %all-gather.4 = bf16[16,4,128]{2,1,0:T(4,128)(2,1)S(1)} all-gather(bf16[1,4,128]{2,1,0:T(4,128)(2,1)S(1)} %convert_bitcast_fusion.1), channel_id=2, replica_groups=mesh['sp'=16,'tp'=2] {'sp'}, dimensions={0}, use_global_device_ids=true | all-gather | bytes 17408 | tf_op jit(solution)/shard_map/all_gather | solution.py:16
  117.5 18.6 %while.67 = (s32[]{:T(128)}, f32[4,128,128]{2,1,0:T(8,128)S(1)}, s32[]{:T(128)}, bf16[16,4,128]{2,1,0:T(4,128)(2,1)S(1)}, bf16[16,4,128,128]{3,2,1,0:T(8,128)(2,...) while((s32[]{:T(128)}, f32[4,128,128]{2,1,0:T(8,128)S(1)}, s32[]{:T(128)}, ...), condition=%wide.region_9.10_spmd.clone, body=%wide.region_8.9_spmd.clone.sunk | while | flops 328200 | bytes 660647 | solution.py:34
  117.6 1.1 fusion.162
  118.7 1.1 fusion.162
  119.9 1.1 fusion.162
  121.1 1.1 fusion.162
  122.2 1.1 fusion.162
  123.4 1.1 fusion.162
  124.5 1.1 fusion.162
  125.7 1.1 fusion.162
  126.9 1.1 fusion.162
  128.0 1.1 fusion.162
  129.2 1.1 fusion.162
  130.4 1.1 fusion.162
  131.5 1.1 fusion.162
  132.7 1.1 fusion.162
  133.9 1.1 fusion.162
  135.0 1.1 fusion.162
  137.2 18.4 %while.65 = (s32[]{:T(128)}, f32[4,128,128]{2,1,0:T(8,128)S(1)}, s32[]{:T(128)}, bf16[16,4,128]{2,1,0:T(4,128)(2,1)S(1)}, bf16[16,4,128,128]{3,2,1,0:T(8,128)(2,1)}, /*index=5*/s32[]{:T(128)}, s32[]{:T(128)}) while((s32[]{:T(128)}, f32[4,128,128]{2,1,0:T(8,128)S(1)}, s32[]{:T(128)}, bf16[16,4,128]{2,1,0:T(4,128)(2,1)S(1)}, ...), condition=%wide.region_4.5_spmd.clone, body=%wide.region_3.4_spmd.clone.sunk | while | flops 328196 | bytes 660585 | solution.py:34
  137.2 1.2 fusion.148
  138.4 1.1 fusion.148
  139.6 1.1 fusion.148
  140.7 1.1 fusion.148
  141.9 1.1 fusion.148
  143.0 1.1 fusion.148
  144.2 1.1 fusion.148
  145.3 1.1 fusion.148
  146.5 1.1 fusion.148
  147.6 1.1 fusion.148
  148.8 1.1 fusion.148
  149.9 1.1 fusion.148
  151.1 1.1 fusion.148
  152.2 1.1 fusion.148
  153.4 1.1 fusion.148
  154.5 1.1 fusion.148
  157.2 3.5 all-to-all-start
  160.8 4.4 all-to-all-done
  165.3 16.2 %all-gather.13.cloned.1.call-done = bf16[1024,2048]{1,0:T(8,128)(2,1)} async-done(((bf16[1024,128]{1,0:T(8,128)(2,1)}), bf16[1024,2048]{1,0:T(8,128)(2,1)}) %all-gather.13.cloned.1.call-update) | async-done | bytes 4194320 | tf_op jit(solution)/shard_map/all_gather | solution.py:138
  181.5 3.2 multiply_reduce_fusion
  184.8 9.1 %all_gather.48 = bf16[128,2048]{1,0:T(8,128)(2,1)S(1)} all-gather(bf16[64,2048]{1,0:T(8,128)(2,1)S(1)} %multiply_convert_fusion), channel_id=1, replica_groups=mesh['sp'=16,'tp'=2] {'tp'}, dimensions={0}, use_global_device_ids=true | all-gather | bytes 786432 | tf_op jit(solution)/shard_map/all_gather | solution.py:169
  193.9 81.9 %all-gather.17.cloned.1.call-done = bf16[2048,2816]{1,0:T(8,128)(2,1)} async-done(((bf16[128,2816]{1,0:T(8,128)(2,1)}), bf16[2048,2816]{1,0:T(8,128)(2,1)}) %all-gather.17.cloned.1.call-update) | async-done | bytes 11534352 | tf_op jit(solution)/shard_map/all_gather | solution.py:136
  275.8 5.9 %convolution_convert_fusion = bf16[128,2816]{1,0:T(8,128)(2,1)S(1)} fusion(bf16[128,2048]{1,0:T(8,128)(2,1)S(1)} %all_gather.48, bf16[2048,2816]{1,0:T(8,128)(2,1)} %all-gather.17.cloned.1.call-done), kind=kOutput, calls=%fused_computation.86 | convolution fusion | flops 1476755456 | bytes 12779520 | tf_op jit(solution)/shard_map/dot_general | solution.py:171
  281.8 88.4 %all-gather.15.cloned.1.call-done = bf16[2048,2816]{1,0:T(8,128)(2,1)} async-done(((bf16[128,2816]{1,0:T(8,128)(2,1)}), bf16[2048,2816]{1,0:T(8,128)(2,1)}) %all-gather.15.cloned.1.call-update) | async-done | bytes 11534352 | tf_op jit(solution)/shard_map/all_gather | solution.py:135
  370.2 5.9 %convolution_convert_fusion.1 = bf16[128,2816]{1,0:T(8,128)(2,1)S(1)} fusion(bf16[128,2048]{1,0:T(8,128)(2,1)S(1)} %all_gather.48, bf16[2048,2816]{1,0:T(8,128)(2,1)} %all-gather.15.cloned.1.call-done), kind=kOutput, calls=%fused_computation.87 | convolution fusion | flops 1476755456 | bytes 12779520 | tf_op jit(solution)/shard_map/dot_general | solution.py:170
  376.2 2.2 collective-permute-start
  378.3 1.3 collective-permute-start.1
  379.8 1.6 collective-permute-done.1
  381.4 3.2 multiply_add_fusion
  384.7 82.9 %all-gather.19.cloned.1.call-done = bf16[2816,2048]{1,0:T(8,128)(2,1)} async-done(((bf16[2816,128]{1,0:T(8,128)(2,1)}), bf16[2816,2048]{1,0:T(8,128)(2,1)}) %all-gather.19.cloned.1.call-update) | async-done | bytes 11534352 | tf_op jit(solution)/shard_map/all_gather | solution.py:137
  467.6 7.7 %convolution_convert_fusion.2 = bf16[128,2048]{1,0:T(8,128)(2,1)} fusion(bf16[2816,2048]{1,0:T(8,128)(2,1)} %all-gather.19.cloned.1.call-done, f32[128,5632]{1,0:T(8,128)} %multiply_add_fusion), kind=kOutput, calls=%fused_computation.89 | convolution fusion | flops 1478819840 | bytes 14942208 | tf_op jit(solution)/shard_map/dot_general | solution.py:182
  475.3 13.0 %reduce-scatter.2.cloned.1.call-done = bf16[64,2048]{1,0:T(8,128)(2,1)} async-done(((bf16[128,2048]{1,0:T(8,128)(2,1)}), bf16[64,2048]{1,0:T(8,128)(2,1)}) %reduce-scatter.2.cloned.1.call-update) | async-done | bytes 262160 | tf_op jit(solution)/shard_map/reduce_scatter | solution.py:183
  488.3 1.7 add_convert_fusion
  (170 shorter events, 19.0 us)
Async XLA Ops:
  6.5 3.2 copy-start.4
  6.5 3.9 copy-start.1
  6.5 111.0 %all-gather.23.cloned.1.call-start = ((), (), s32[]{:S(2)}) async-start(), calls=%async_computation.8 | async-start | bytes 2228224 | tf_op jit(solution)/shard_map/all_gather | solution.py:16
  10.7 31.6 %copy-start.2 = (bf16[128,512]{1,0:T(8,128)(2,1)S(1)}, bf16[128,512]{1,0:T(8,128)(2,1)}, u32[]{:S(2)}) copy-start(bf16[128,512]{1,0:T(8,128)(2,1)} %param.25) | copy-start | bytes 393220
  41.3 95.8 %all-gather.21.cloned.1.call-start = ((), (), s32[]{:S(2)}) async-start(), calls=%async_computation.7 | async-start | bytes 2228224 | tf_op jit(solution)/shard_map/all_gather | solution.py:16
  72.9 3.5 copy-start.3
  72.9 44.6 %copy-start.5 = (f32[3,2816]{1,0:T(4,128)S(1)}, f32[3,2816]{1,0:T(4,128)}, u32[]{:S(2)}) copy-start(f32[3,2816]{1,0:T(4,128)} %param.37) | copy-start | bytes 101380
  73.6 107.8 %all-gather.13.cloned.1.call-start = ((), (), s32[]{:S(2)}) async-start(), calls=%async_computation.2 | async-start | bytes 4456448 | tf_op jit(solution)/shard_map/all_gather | solution.py:138
  74.4 201.4 %all-gather.17.cloned.1.call-start = ((), (), s32[]{:S(2)}) async-start(), calls=%async_computation.4 | async-start | bytes 12255232 | tf_op jit(solution)/shard_map/all_gather | solution.py:136
  74.9 295.2 %all-gather.15.cloned.1.call-start = ((), (), s32[]{:S(2)}) async-start(), calls=%async_computation.3 | async-start | bytes 12255232 | tf_op jit(solution)/shard_map/all_gather | solution.py:135
  75.5 392.1 %all-gather.19.cloned.1.call-start = ((), (), s32[]{:S(2)}) async-start(), calls=%async_computation.5 | async-start | bytes 12255232 | tf_op jit(solution)/shard_map/all_gather | solution.py:137
  136.8 19.5 %copy-start.8 = (f32[128]{0:T(128)S(1)}, f32[128]{0:T(128)}, u32[]{:S(2)}) copy-start(f32[128]{0:T(128)} %param.32) | copy-start | bytes 1540
  137.2 23.6 %copy-start.6 = (f32[3,2816]{1,0:T(4,128)S(1)}, f32[3,2816]{1,0:T(4,128)}, u32[]{:S(2)}) copy-start(f32[3,2816]{1,0:T(4,128)} %param.38) | copy-start | bytes 101380
  137.2 44.3 %copy-start = (bf16[64,2048]{1,0:T(8,128)(2,1)S(1)}, bf16[64,2048]{1,0:T(8,128)(2,1)}, u32[]{:S(2)}) copy-start(bf16[64,2048]{1,0:T(8,128)(2,1)} %param.24) | copy-start | bytes 786436
  157.2 27.4 %copy-start.7 = (f32[2048]{0:T(1024)S(1)}, f32[2048]{0:T(1024)}, u32[]{:S(2)}) copy-start(f32[2048]{0:T(1024)} %param.34) | copy-start | bytes 24580
  157.2 8.0 %all-to-all-start = ((bf16[2,64,512]{2,1,0:T(8,128)(2,1)}), bf16[2,64,512]{2,1,0:T(8,128)(2,1)S(1)}, u32[]{:S(2)}, u32[]{:S(2)}) async-start(bf16[2,64,512]{2,1,0:T(8,128)(2,1)} %convert_element_type.128), calls=%async_computation | async-start | bytes 262144 | tf_op jit(solution)/shard_map/all_to_all | solution.py:165
  160.8 327.5 %reduce-scatter.2.cloned.1.call-start = ((), (), s32[]{:S(2)}) async-start(), calls=%async_computation.6 | async-start | bytes 786432 | tf_op jit(solution)/shard_map/reduce_scatter | solution.py:183
  376.2 3.7 collective-permute-start
  378.3 3.1 collective-permute-start.1
Sparse Core Ops, SparseCore 0:
  41.5 44.2 all-gather.22
  87.9 40.1 all-gather.20
  130.2 51.1 all-gather.12
  183.6 92.1 all-gather.16
  277.9 92.2 all-gather.14
  372.2 95.3 all-gather.18
  475.4 12.7 reduce-scatter.1
where the time goes:
time: 498 us; the launch traced here: 497 us
  waiting for transfers between devices  291 us (58%)
  other arithmetic  98.2 us (20%)
  blocking collectives  50 us (10%)
  matrix products  29.6 us (6%)
  between operations  14 us (3%)
  starting transfers between devices  7.38 us (1%)
  local copies, waits for them, and re-layouts  5.26 us (1%)
    all_gather x1, waiting for transfers between devices, on_device(): lax.all_gather(gate_up_matrix, 'sp', axis=0, tiled=True)  88.4 us
    all_gather x1, waiting for transfers between devices, on_device(): lax.all_gather(down_matrix, 'sp', axis=1, tiled=True)  82.9 us
    all_gather x1, waiting for transfers between devices, on_device(): lax.all_gather(value_up_matrix, 'sp', axis=0, tiled=True)  81.9 us
    all_gather x2, blocking collectives, carried_in(): lax.all_gather(part.astype(kind), axis)  40.8 us
    select_n x32, other arithmetic, hop(): return jax.tree.map(lambda a, b: jnp.where(reached, a, b), new, before)  35.4 us
    dot_general x4, other arithmetic, advance(): jnp.einsum('ihd,jhd,ijhd->hij', query_part, key_part, jnp.exp(gaps), prec...  29.1 us
    while x4, other arithmetic  23.5 us
    all_gather x1, waiting for transfers between devices, on_device(): lax.all_gather(output_matrix, 'sp', axis=1, tiled=True)  16.2 us
  transfers between devices with their start and end apart: 10, of which 7 were waited for; matrix products, arithmetic and copies ran while one was open for 18% of the time, Pallas kernels for 0%

commit v1 on v0

v1 whole, which is shorter than its diff:
```python
import functools
import math

import jax
import jax.numpy as jnp
from jax import lax
from jax.experimental import pallas as pl
from jax.experimental.pallas import tpu as pltpu
from jax.sharding import PartitionSpec as P

HEAD_WIDTH = 128
EPSILON = 1e-06
MESH = pl.DeviceIdType.MESH
F32 = jnp.float32
BF16 = jnp.bfloat16
DECAY_ROWS = 16


class Grid:
    def __init__(self, mesh):
        sp, tp = mesh.shape["sp"], mesh.shape["tp"]
        self.sp, self.x = sp, tp
        self.c = math.gcd(sp, 2)
        self.y = math.gcd(sp // self.c, 2)
        self.z = sp // (self.c * self.y)
        self.ids = iter(range(100))

    def size(self, dim):
        return getattr(self, dim)

    def place(self):
        s, t = lax.axis_index("sp"), lax.axis_index("tp")
        return {
            "sp": s,
            "x": t,
            "c": lax.rem(s, self.c),
            "y": lax.rem(s // self.c, self.y),
            "z": s // (self.c * self.y),
        }

    def peer(self, place, dim, index):
        if dim == "sp":
            return {"sp": index, "tp": place["x"]}
        at = dict(place)
        at[dim] = index
        return {"sp": (at["z"] * self.y + at["y"]) * self.c + at["c"], "tp": at["x"]}

    def greet(self, place, dims):
        barrier = pltpu.get_barrier_semaphore()
        count = 0
        for dim in dims:
            n = self.size(dim)
            for k in range(1, n):
                peer = self.peer(place, dim, lax.rem(place[dim] + k, n))
                pl.semaphore_signal(barrier, inc=1, device_id=peer, device_id_type=MESH)
                count += 1
        pl.semaphore_wait(barrier, count)


def exchange_kernel(grid, dims, keep, *refs):
    m = len(dims)
    ins, outs = refs[:m], refs[m : 2 * m]
    send_sem, recv_sem, own_sem = refs[2 * m :]
    place = grid.place()
    copies = []
    grid.greet(place, sorted(set(dims)))
    base = 0
    for i, dim in enumerate(dims):
        n, me = grid.size(dim), place[dim]
        for k in range(1, n):
            to = lax.rem(me + k, n)
            slot = me if keep else k - 1
            copy = pltpu.make_async_remote_copy(
                src_ref=ins[i].at[to],
                dst_ref=outs[i].at[slot],
                send_sem=send_sem.at[base + k - 1],
                recv_sem=recv_sem.at[base + k - 1],
                device_id=grid.peer(place, dim, to),
                device_id_type=MESH,
            )
            copy.start()
            copies.append(copy)
        base += n - 1
    if keep:
        for i, dim in enumerate(dims):
            me = place[dim]
            own = pltpu.make_async_copy(ins[i].at[me], outs[i].at[me], own_sem.at[i])
            own.start()
            copies.append(own)
    for copy in copies:
        copy.wait()


def exchange(grid, items, keep):
    dims = tuple(d for _, d in items)
    total = sum(grid.size(d) - 1 for d in dims)
    shapes = tuple(
        jax.ShapeDtypeStruct(a.shape if keep else (a.shape[0] - 1,) + a.shape[1:], a.dtype)
        for a, _ in items
    )
    return pl.pallas_call(
        functools.partial(exchange_kernel, grid, dims, keep),
        out_shape=shapes,
        in_specs=[pl.BlockSpec(memory_space=pl.ANY)] * len(items),
        out_specs=[pl.BlockSpec(memory_space=pl.ANY)] * len(items),
        scratch_shapes=[
            pltpu.SemaphoreType.DMA((total,)),
            pltpu.SemaphoreType.DMA((total,)),
            pltpu.SemaphoreType.DMA((len(items),)),
        ],
        compiler_params=pltpu.CompilerParams(
            collective_id=next(grid.ids), has_side_effects=True
        ),
    )(*[a for a, _ in items])


def gather_kernel(grid, x_ref, out_ref, send_sem, recv_sem, own_sem):
    place = grid.place()
    z, y, c, x = (place[d] for d in "zycx")
    half = x_ref.shape[1] // 2
    first, second = pl.ds(0, half), pl.ds(half, half)
    everything = slice(None)
    grid.greet(place, ("z", "y", "c", "x"))
    own = pltpu.make_async_copy(x_ref, out_ref.at[z, y, c, x], own_sem)
    own.start()
    used = 0

    def push(dim, src, dst):
        nonlocal used
        n, copies = grid.size(dim), []
        for k in range(1, n):
            copy = pltpu.make_async_remote_copy(
                src_ref=src,
                dst_ref=dst,
                send_sem=send_sem.at[used],
                recv_sem=recv_sem.at[used],
                device_id=grid.peer(place, dim, lax.rem(place[dim] + k, n)),
                device_id_type=MESH,
            )
            copy.start()
            copies.append(copy)
            used += 1
        return copies

    stage = push("z", x_ref, out_ref.at[z, y, c, x])
    own.wait()
    for copy in stage:
        copy.wait()
    a = out_ref.at[:, y, c, x, :, first]
    b = out_ref.at[:, y, c, x, :, second]
    stage = push("y", a, a) + push("x", b, b)
    for copy in stage:
        copy.wait()
    a = out_ref.at[:, :, c, x, :, first]
    b = out_ref.at[:, y, c, :, :, second]
    stage = push("x", a, a) + push("y", b, b)
    for copy in stage:
        copy.wait()
    a = out_ref.at[:, :, c]
    for copy in push("c", a, a):
        copy.wait()


def gather(grid, array):
    total = sum(grid.size(d) - 1 for d in "zyyxxc")
    return pl.pallas_call(
        functools.partial(gather_kernel, grid),
        out_shape=jax.ShapeDtypeStruct(
            (grid.z, grid.y, grid.c, grid.x) + array.shape, array.dtype
        ),
        in_specs=[pl.BlockSpec(memory_space=pltpu.VMEM)],
        out_specs=pl.BlockSpec(memory_space=pl.ANY),
        scratch_shapes=[
            pltpu.SemaphoreType.DMA((total,)),
            pltpu.SemaphoreType.DMA((total,)),
            pltpu.SemaphoreType.DMA,
        ],
        compiler_params=pltpu.CompilerParams(
            collective_id=next(grid.ids), has_side_effects=True
        ),
    )(array)


def reduce_scatter(grid, first, second):
    place = grid.place()

    def stage(items):
        got = exchange(grid, items, False)
        sums = []
        for (array, dim), other in zip(items, got):
            own = lax.dynamic_index_in_dim(array, place[dim], 0, keepdims=False)
            sums.append(own.astype(F32) + jnp.sum(other.astype(F32), axis=0))
        return sums

    for dims in ("cc", "xy", "yx", "zz"):
        first, second = stage([(first.astype(BF16), dims[0]), (second.astype(BF16), dims[1])])
    return jnp.concatenate([first, second], axis=-1)


def dot(a, b, dims, precision=None):
    return lax.dot_general(
        a, b, (dims, ((), ())), precision=precision, preferred_element_type=F32
    )


def local_kernel(
    heads, zf_ref, zb_ref, v_ref, q_ref, floor_ref, extra_ref, out_ref, carry_ref, state_ref, decay_ref
):
    length = v_ref.shape[0]
    rows = lax.broadcasted_iota(jnp.int32, (length, length), 0)
    cols = lax.broadcasted_iota(jnp.int32, (length, length), 1)
    middle = length // 2
    for h in range(heads):
        at = slice(h * HEAD_WIDTH, (h + 1) * HEAD_WIDTH)
        values = v_ref[:, at]
        logits = q_ref[:, at].astype(F32)
        queries = logits * jax.nn.sigmoid(logits)
        scores = jnp.zeros((length, length), F32)
        for d, z_ref in enumerate((zf_ref, zb_ref)):
            mask = rows >= cols if d == 0 else rows <= cols
            z = z_ref[:, at].astype(F32)
            floor = floor_ref[d : d + 1, at]
            rest = 1.0 - floor
            logf = jnp.log(floor + rest * jax.nn.sigmoid(z)) + extra_ref[d, :, h : h + 1]
            key = rest * jax.nn.sigmoid(-z)
            running = dot(
                jnp.where(mask, 1.0, 0.0), logf, ((1,), (0,)), lax.Precision.HIGHEST
            )
            last = length - 1 if d == 0 else 0
            total = running[last : last + 1]
            centred = running - running[middle : middle + 1]
            part = dot(
                (queries * jnp.exp(centred)).astype(BF16),
                (key * jnp.exp(-centred)).astype(BF16),
                ((1,), (1,)),
            )
            scores += jnp.where(mask, part, 0.0)
            carry_ref[d, :, at] = (queries * jnp.exp(running)).astype(BF16)
            fresh = (key * jnp.exp(total - running)).astype(BF16)
            state_ref[d, h] = dot(values, fresh, ((0,), (0,))).astype(BF16)
            decay_ref[d, h] = jnp.broadcast_to(
                jnp.exp(total), (DECAY_ROWS, HEAD_WIDTH)
            ).astype(BF16)
        out_ref[:, at] = dot(scores.astype(BF16), values, ((1,), (0,)))


def prefix_kernel(rows, got_ref, out_ref):
    n = got_ref.shape[0]
    forward = lax.axis_index("sp") < n // 2

    def hop(k, carry):
        at = jnp.where(forward, k, n - 1 - k)
        out_ref[at] = carry.astype(BF16)
        block = got_ref[at].astype(F32)
        return block[rows : rows + 1] * carry + block[:rows]

    lax.fori_loop(0, n, hop, jnp.zeros((rows, HEAD_WIDTH), F32))


def finish_kernel(heads, out_ref, carry_ref, enter_ref, gate_ref, scale_ref, gated_ref):
    for h in range(heads):
        at = slice(h * HEAD_WIDTH, (h + 1) * HEAD_WIDTH)
        total = out_ref[:, at]
        for d in range(2):
            total += dot(carry_ref[d, :, at], enter_ref[d, h], ((1,), (1,)))
        mean = jnp.mean(total * total, axis=-1, keepdims=True)
        g = gate_ref[:, at].astype(F32)
        gated_ref[:, at] = (
            total * lax.rsqrt(mean + EPSILON) * scale_ref[...] * (g * jax.nn.sigmoid(g))
        ).astype(BF16)


def on_device(
    grid,
    residual,
    forget_forward,
    forget_backward,
    value_written,
    query_logits,
    output_gate_logits,
    forget_minimum,
    extra_log_rate,
    head_norm_scale,
    output_matrix,
    prenorm_scale,
    gate_up_matrix,
    value_up_matrix,
    gate_taps,
    value_taps,
    down_matrix,
):
    sp, tp = grid.sp, grid.x
    length, width = value_written.shape
    heads = width // HEAD_WIDTH
    depth, units = gate_up_matrix.shape
    unit = units // sp
    me = lax.axis_index("sp")

    out_full = lax.all_gather(output_matrix, "sp", axis=1, tiled=True)

    def cut(w):
        return w.reshape(depth, sp, unit).transpose(1, 0, 2)

    up = jnp.concatenate([cut(gate_up_matrix), cut(value_up_matrix)], axis=2)
    down = down_matrix.reshape(sp, unit, down_matrix.shape[1])
    up, down = exchange(grid, [(up, "sp"), (down, "sp")], True)
    up = up.reshape(sp * depth, 2 * unit)
    down = down.transpose(1, 0, 2).reshape(unit, -1)

    local, carry, state, decay = pl.pallas_call(
        functools.partial(local_kernel, heads),
        out_shape=(
            jax.ShapeDtypeStruct((length, width), F32),
            jax.ShapeDtypeStruct((2, length, width), BF16),
            jax.ShapeDtypeStruct((2, heads, HEAD_WIDTH, HEAD_WIDTH), BF16),
            jax.ShapeDtypeStruct((2, heads, DECAY_ROWS, HEAD_WIDTH), BF16),
        ),
    )(forget_forward, forget_backward, value_written, query_logits, forget_minimum, extra_log_rate)

    rows = 2 * heads * HEAD_WIDTH // sp
    decays = jnp.repeat(
        decay.reshape(2 * heads, DECAY_ROWS, HEAD_WIDTH), sp // (2 * heads), axis=0
    )
    message = jnp.concatenate([state.reshape(sp, rows, HEAD_WIDTH), decays], axis=1)
    (got,) = exchange(grid, [(message, "sp")], True)
    prefix = pl.pallas_call(
        functools.partial(prefix_kernel, rows),
        out_shape=jax.ShapeDtypeStruct((sp, rows, HEAD_WIDTH), BF16),
    )(got)
    (entering,) = exchange(grid, [(prefix, "sp")], True)
    gated = pl.pallas_call(
        functools.partial(finish_kernel, heads),
        out_shape=jax.ShapeDtypeStruct((length, width), BF16),
    )(
        local,
        carry,
        entering.reshape(2, heads, HEAD_WIDTH, HEAD_WIDTH),
        output_gate_logits,
        head_norm_scale[None],
    )
    (swapped,) = exchange(grid, [(gated.reshape(tp, length // tp, width), "x")], True)
    token_rows = swapped.transpose(1, 0, 2).reshape(length // tp, tp * width)
    mixed = jnp.dot(token_rows, out_full, preferred_element_type=F32)
    own_after = residual.astype(F32) + mixed
    mean = jnp.mean(own_after * own_after, axis=-1, keepdims=True)
    normed = (own_after * lax.rsqrt(mean + EPSILON) * prenorm_scale).astype(BF16)
    everyone = gather(grid, normed)
    tokens = everyone.reshape(-1, normed.shape[1])
    upward = jnp.dot(tokens, up, preferred_element_type=F32).astype(BF16)
    padded = jnp.pad(upward, ((1, 1), (0, 0)))
    taps = jnp.concatenate(
        [
            lax.dynamic_slice_in_dim(gate_taps, me * unit, unit, 1),
            lax.dynamic_slice_in_dim(value_taps, me * unit, unit, 1),
        ],
        axis=1,
    )
    count = tokens.shape[0]
    conv = padded[:count] * taps[0] + padded[1 : count + 1] * taps[1] + padded[2:] * taps[2]
    hidden = (jax.nn.silu(conv[:, :unit]) * conv[:, unit:]).astype(BF16)
    parts = hidden.reshape(everyone.shape[:-1] + (unit,))
    half = down.shape[1] // 2

    def project(order, weights):
        moved = parts.transpose(*order, 4, 5)
        product = jnp.dot(moved.reshape(-1, unit), weights, preferred_element_type=F32)
        return product.astype(BF16).reshape(moved.shape[:-1] + (weights.shape[1],))

    down_sum = reduce_scatter(
        grid, project((2, 3, 1, 0), down[:, :half]), project((2, 1, 3, 0), down[:, half:])
    )
    return (own_after + down_sum).astype(BF16)


def solution(mesh):
    return jax.shard_map(
        functools.partial(on_device, Grid(mesh)),
        mesh=mesh,
        in_specs=(
            P(("sp", "tp"), None),
            P("sp", "tp"),
            P("sp", "tp"),
            P("sp", "tp"),
            P("sp", "tp"),
            P("sp", "tp"),
            P(None, "tp"),
            P(None, "sp", "tp"),
            P(),
            P(None, "sp"),
            P(),
            P("sp", "tp"),
            P("sp", "tp"),
            P(None, "tp"),
            P(None, "tp"),
            P("tp", "sp"),
        ),
        out_specs=P(("sp", "tp"), None),
        check_vma=False,
    )
```

time: 498 us -> 312 us (0.63)
  waiting for transfers between devices: 291 us -> 0.73 us
  Pallas kernels: 0 us -> 244 us
  other arithmetic: 98.2 us -> 28 us
  blocking collectives: 50 us -> 0 us
  matrix products: 29.6 us -> 16.6 us
  starting transfers between devices: 7.38 us -> 0.01 us
    all_gather x6 -> x1, waiting for transfers between devices: 269 us -> 0.02 us  [on_device(): out_full = lax.all_gather(output_matrix, 'sp', axis=1, tiled=True)]
    pallas_call x0 -> x12, Pallas kernels: none -> 244 us  [the longest x8 165 us: exchange(): pl.pallas_call(functools.partial(exchange_kernel, grid, dims, keep), out_...]
    all_gather x3 -> x0, blocking collectives: 50 us -> none  [the longest x2 40.8 us: carried_in(): lax.all_gather(part.astype(kind), axis)]
    select_n x32 -> x0, other arithmetic: 35.4 us -> none  [hop(): return jax.tree.map(lambda a, b: jnp.where(reached, a, b), new, before)]
    dot_general x4 -> x0, other arithmetic: 29.1 us -> none  [advance(): jnp.einsum('ihd,jhd,ijhd->hij', query_part, key_part, jnp.exp(gaps), prec...]
    while x4 -> x0, other arithmetic: 23.5 us -> none
    convert_element_type x6 -> x9, other arithmetic: 3.27 us -> 17.5 us  [the longest x3 9.62 us: reduce_scatter(): second.astype(BF16)]
    dot_general x18 -> x4, matrix products: 29.6 us -> 16.6 us  [the longest x1 6.99 us: on_device(): upward = jnp.dot(tokens, up, preferred_element_type=F32).astype(BF16)]
  transfers between devices with their start and end apart: 10 -> 1, of which waited for: 7 -> 0; matrix products, arithmetic and copies ran while one was open for 18% -> 4% of each run, Pallas kernels for 0% -> 31%
where the time goes in v1:
time: 312 us
  Pallas kernels  244 us (78%)
  other arithmetic  28 us (9%)
  matrix products  16.6 us (5%)
  between operations  13.7 us (4%)
  local copies, waits for them, and re-layouts  8.48 us (3%)
    pallas_call x8, Pallas kernels, exchange(): pl.pallas_call(functools.partial(exchange_kernel, grid, dims, keep), out_...  165 us
    pallas_call x1, Pallas kernels, gather(): pl.pallas_call(functools.partial(gather_kernel, grid), out_shape=jax.Shap...  71.3 us
    convert_element_type x3, other arithmetic, reduce_scatter(): second.astype(BF16)  9.62 us
    dot_general x1, matrix products, on_device(): upward = jnp.dot(tokens, up, preferred_element_type=F32).astype(BF16)  6.99 us
    dot_general x2, matrix products, project(): jnp.dot(moved.reshape(-1, unit), weights, preferred_element_type=F32)  6.41 us
  transfers between devices with their start and end apart: 1, of which 0 were waited for; matrix products, arithmetic and copies ran while one was open for 4% of the time, Pallas kernels for 31%

profile of v1, /device:TPU:0, one launch (start us, length us, event | category | flops | bytes accessed | tf_op | source)
XLA Modules:
  0.0 311.6 jit_solution(13440009049636709072)
XLA Ops:
  6.5 0.0 all-gather.2.cloned.1.call-start
  6.5 0.7 all-gather.2.cloned.1.call-update
  7.3 1.5 copy.18.extra_ref
  8.8 4.2 %shard_map.154 = (f32[128,512]{1,0:T(8,128)}, bf16[2,128,512]{2,1,0:T(8,128)(2,1)}, bf16[2,4,128,128]{3,2,1,0:T(8,128)(2,1)}, bf16[2,4,16,128]{3,2,1,0:T(8,128)(2,1)}) custom-call(bf16[128,512]{1,0:T(8,128)(2,1)} %zf_ref.1, bf16[128,512]{1,0:T(8,128)(2,1)} %zb_ref.1, bf16[128,512]{1,0:T(8,128)(2,1)} %v_ref.1, bf16[128,512]{1,0:T(8,128)(2,1)} %q_ref.1, ...), custom_call_target="tpu_custom_call" | custom-call | tf_op jit(solution)/shard_map/pallas_call | solution.py:310
  13.0 0.8 broadcast_in_dim.8
  13.8 1.7 pad_maximum_fusion.1.refs_0_
  15.5 13.9 %shard_map.155.got_ref = bf16[16,80,128]{2,1,0:T(8,128)(2,1)} custom-call(bf16[16,80,128]{2,1,0:T(8,128)(2,1)} %pad_maximum_fusion.1.refs_0_), custom_call_target="tpu_custom_call" | custom-call | tf_op jit(solution)/shard_map/pallas_call | solution.py:101
  29.4 1.8 shard_map.156.refs_0_
  31.2 17.9 %shard_map.157 = bf16[16,64,128]{2,1,0:T(8,128)(2,1)} custom-call(bf16[16,64,128]{2,1,0:T(8,128)(2,1)} %shard_map.156.refs_0_), custom_call_target="tpu_custom_call" | custom-call | tf_op jit(solution)/shard_map/pallas_call | solution.py:101
  49.1 2.2 shard_map.158
  51.3 4.6 %shard_map.159 = bf16[2,64,512]{2,1,0:T(8,128)(2,1)} custom-call(bf16[2,64,512]{2,1,0:T(8,128)(2,1)} %bitcast.83), custom_call_target="tpu_custom_call" | custom-call | tf_op jit(solution)/shard_map/pallas_call | solution.py:101
  56.0 1.6 copy.28
  57.5 0.0 copy-done.7
  57.5 0.3 copy.20
  57.9 0.5 copy.21
  58.4 0.0 copy-done.8
  58.4 0.3 copy.22
  58.8 0.5 copy.23
  59.3 1.8 pad_maximum_fusion.refs_0_
  61.1 52.5 %shard_map.161 = (bf16[16,128,352]{2,1,0:T(8,128)(2,1)}, bf16[16,176,128]{2,1,0:T(8,128)(2,1)}) custom-call(bf16[16,128,352]{2,1,0:T(8,128)(2,1)} %pad_maximum_fusion.refs_0_, bf16[16,176,128]{2,1,0:T(8,128)(2,1)} %bitcast.81), custom_call_target="tpu_custom_call" | custom-call | tf_op jit(solution)/shard_map/pallas_call | solution.py:101
  113.6 0.8 constant_dynamic-slice_fusion
  114.4 0.1 maximum_reduce_fusion.1
  114.5 1.2 copy_bitcast_fusion
  115.7 0.0 all-gather.2.cloned.1.call-done
  115.7 0.0 copy-done.9
  115.7 0.0 copy-done.10
  115.7 0.0 copy-start.11
  115.7 3.2 %multiply_reduce_fusion = (f32[64]{0:T(128)S(1)}, f32[64,2048]{1,0:T(8,128)S(1)}) fusion(bf16[64,1024]{1,0:T(8,128)(2,1)S(1)} %bitcast.84, bf16[1024,2048]{1,0:T(8,128)(2,1)} %all-gather.2.cloned.1.call-done, bf16[64,2048]{1,0:T(8,128)(2,1)S(1)} %copy-done.10), kind=kOutput, calls=%fused_computation.24 | convolution fusion | flops 268959680 | bytes 5112064 | tf_op jit(solution)/shard_map/dot_general | solution.py:343
  118.9 0.0 copy-done.11
  118.9 0.8 multiply_convert_fusion.x_ref
  119.7 71.3 %shard_map.160 = bf16[4,2,2,2,64,2048]{5,4,3,2,1,0:T(8,128)(2,1)} custom-call(bf16[64,2048]{1,0:T(8,128)(2,1)} %multiply_convert_fusion.x_ref), custom_call_target="tpu_custom_call" | custom-call | tf_op jit(solution)/shard_map/pallas_call | solution.py:166
  191.1 7.0 %convolution_convert_fusion.2 = bf16[2048,352]{0,1:T(8,128)(2,1)S(1)} fusion(bf16[2048,2048]{1,0:T(8,128)(2,1)} %bitcast.69, bf16[2048,352]{1,0:T(8,128)(2,1)} %bitcast.89), kind=kOutput, calls=%fused_computation.5 | convolution fusion | flops 2953510912 | bytes 11272192 | tf_op jit(solution)/shard_map/dot_general | solution.py:349
  198.1 2.8 multiply_add_fusion
  200.9 0.4 fusion.2
  201.3 0.7 copy.24
  202.1 0.1 copy.27
  202.1 0.1 copy.25
  202.2 3.2 %convolution_convert_fusion.1 = bf16[2048,1024]{1,0:T(8,128)(2,1)} fusion(bf16[2048,176]{1,0:T(8,128)(2,1)S(1)} %bitcast.71, bf16[176,2048]{1,0:T(8,128)(2,1)S(1)} %copy_bitcast_fusion), kind=kOutput, calls=%fused_computation.3 | convolution fusion | flops 740294656 | bytes 5603328 | tf_op jit(solution)/shard_map/dot_general | solution.py:366
  205.4 3.2 %convolution_convert_fusion = bf16[2048,1024]{1,0:T(8,128)(2,1)} fusion(bf16[2048,176]{1,0:T(8,128)(2,1)S(1)} %bitcast.70, bf16[176,2048]{1,0:T(8,128)(2,1)S(1)} %copy_bitcast_fusion), kind=kOutput, calls=%fused_computation.2 | convolution fusion | flops 740294656 | bytes 5603328 | tf_op jit(solution)/shard_map/dot_general | solution.py:366
  208.6 7.6 %shard_map.162 = (bf16[1,2,2,4,64,1024]{5,4,3,2,1,0:T(8,128)(2,1)}, bf16[1,2,2,4,64,1024]{5,4,3,2,1,0:T(8,128)(2,1)}) custom-call(bf16[2,2,2,4,64,1024]{5,4,3,2,1,0:T(8,128)(2,1)} %bitcast.61, bf16[2,2,2,4,64,1024]{5,4,3,2,1,0:T(8,128)(2,1)} %bitcast.63), custom_call_target="tpu_custom_call" | custom-call | tf_op jit(solution)/shard_map/pallas_call | solution.py:101
  216.2 0.0 copy-start
  216.2 0.0 copy-start.5
  216.2 4.8 %add_convert_fusion = bf16[1,2,2,4,64,1024]{5,4,3,2,1,0:T(8,128)(2,1)} fusion(bf16[1,2,2,4,64,1024]{5,4,3,2,1,0:T(8,128)(2,1)} %get-tuple-element.26, bf16[2,2,2,4,64,1024]{5,4,3,2,1,0:T(8,128)(2,1)} %bitcast.64, s32[]{:T(128)S(6)} %select_n.33), kind=kLoop, calls=%fused_computation | loop fusion | flops 4194304 | bytes 6291460 | tf_op jit(solution)/shard_map/convert_element_type | solution.py:196
  221.0 0.0 copy-done
  221.0 0.0 copy-done.5
  221.0 2.4 add_convert_fusion.1
  223.4 25.8 %shard_map.163 = (bf16[1,2,4,64,1024]{4,3,2,1,0:T(8,128)(2,1)}, bf16[1,2,4,64,1024]{4,3,2,1,0:T(8,128)(2,1)}) custom-call(bf16[2,2,4,64,1024]{4,3,2,1,0:T(8,128)(2,1)} %bitcast.66, bf16[2,2,4,64,1024]{4,3,2,1,0:T(8,128)(2,1)} %bitcast.65), custom_call_target="tpu_custom_call" | custom-call | tf_op jit(solution)/shard_map/pallas_call | solution.py:101
  249.2 0.0 copy-start.2
  249.3 0.0 copy-start.6
  249.3 0.0 copy-done.1
  249.3 2.8 fusion
  252.1 0.0 copy-done.2
  252.1 0.0 copy-done.6
  252.1 1.4 fusion.1
  253.5 13.7 %shard_map.164 = (bf16[1,4,64,1024]{3,2,1,0:T(8,128)(2,1)}, bf16[1,4,64,1024]{3,2,1,0:T(8,128)(2,1)}) custom-call(bf16[2,4,64,1024]{3,2,1,0:T(8,128)(2,1)} %bitcast.72, bf16[2,4,64,1024]{3,2,1,0:T(8,128)(2,1)} %bitcast.73), custom_call_target="tpu_custom_call" | custom-call | tf_op jit(solution)/shard_map/pallas_call | solution.py:101
  267.2 0.0 copy-done.4
  267.2 2.0 fusion.3
  269.3 2.0 fusion.4
  271.3 28.6 %shard_map.165 = (bf16[3,64,1024]{2,1,0:T(8,128)(2,1)}, bf16[3,64,1024]{2,1,0:T(8,128)(2,1)}) custom-call(bf16[4,64,1024]{2,1,0:T(8,128)(2,1)} %bitcast.79, bf16[4,64,1024]{2,1,0:T(8,128)(2,1)} %bitcast.78), custom_call_target="tpu_custom_call" | custom-call | tf_op jit(solution)/shard_map/pallas_call | solution.py:101
  299.9 1.1 convert_reduce_fusion.1
  301.0 1.1 convert_reduce_fusion
  302.1 0.9 convert_add_fusion.5
  303.0 0.9 convert_add_fusion.4
  303.9 0.8 fusion.5
  (9 shorter events, 0.0 us)
Async XLA Ops:
  6.5 109.2 %all-gather.2.cloned.1.call-start = ((), (), s32[]{:S(2)}) async-start(), calls=%async_computation | async-start | bytes 4456448 | tf_op jit(solution)/shard_map/all_gather | solution.py:299
  13.0 44.6 %copy-start.7 = (bf16[128,2816]{1,0:T(8,128)(2,1)S(1)}, bf16[128,2816]{1,0:T(8,128)(2,1)}, u32[]{:S(2)}) copy-start(bf16[128,2816]{1,0:T(8,128)(2,1)} %param.27) | copy-start | bytes 2162692
  51.3 7.1 %copy-start.8 = (bf16[128,2816]{1,0:T(8,128)(2,1)S(1)}, bf16[128,2816]{1,0:T(8,128)(2,1)}, u32[]{:S(2)}) copy-start(bf16[128,2816]{1,0:T(8,128)(2,1)} %param.28) | copy-start | bytes 2162692
  61.1 54.6 %copy-start.9 = (bf16[2,8,8,512]{3,2,0,1:T(8,128)(2,1)S(1)}, bf16[2,8,8,512]{3,2,0,1:T(8,128)(2,1)}, u32[]{:S(2)}) copy-start(bf16[2,8,8,512]{3,2,0,1:T(8,128)(2,1)} %copy.28) | copy-start | bytes 393220
  61.1 54.6 %copy-start.10 = (bf16[64,2048]{1,0:T(8,128)(2,1)S(1)}, bf16[64,2048]{1,0:T(8,128)(2,1)}, u32[]{:S(2)}) copy-start(bf16[64,2048]{1,0:T(8,128)(2,1)} %param.16) | copy-start | bytes 786436
  115.7 3.2 %copy-start.11 = (f32[2048]{0:T(1024)S(1)}, f32[2048]{0:T(1024)}, u32[]{:S(2)}) copy-start(f32[2048]{0:T(1024)} %param.26) | copy-start | bytes 24580
  216.2 4.8 %copy-start = (bf16[2048,1024]{1,0:T(8,128)(2,1)S(1)}, bf16[2048,1024]{1,0:T(8,128)(2,1)}, u32[]{:S(2)}) copy-start(bf16[2048,1024]{1,0:T(8,128)(2,1)} %convolution_convert_fusion.1) | copy-start | bytes 12582916
  216.2 4.8 %copy-start.5 = (bf16[1,2,2,4,64,1024]{5,4,3,2,1,0:T(8,128)(2,1)S(1)}, bf16[1,2,2,4,64,1024]{5,4,3,2,1,0:T(8,128)(2,1)}, u32[]{:S(2)}) copy-start(bf16[1,2,2,4,64,1024]{5,4,3,2,1,0:T(8,128)(2,1)} %get-tuple-element.25) | copy-start | bytes 6291460
  223.4 25.8 %copy-start.1 = (bf16[1,2,2,4,64,1024]{5,4,3,2,1,0:T(8,128)(2,1)S(1)}, bf16[1,2,2,4,64,1024]{5,4,3,2,1,0:T(8,128)(2,1)}, u32[]{:S(2)}) copy-start(bf16[1,2,2,4,64,1024]{5,4,3,2,1,0:T(8,128)(2,1)} %add_convert_fusion) | copy-start | bytes 6291460
  249.2 2.8 copy-start.2
  249.3 2.8 copy-start.6
  252.1 15.1 %copy-start.4 = (bf16[1,2,4,64,1024]{4,3,2,1,0:T(8,128)(2,1)S(1)}, bf16[1,2,4,64,1024]{4,3,2,1,0:T(8,128)(2,1)}, u32[]{:S(2)}) copy-start(bf16[1,2,4,64,1024]{4,3,2,1,0:T(8,128)(2,1)} %fusion) | copy-start | bytes 3145732
  253.5 15.8 %copy-start.3 = (bf16[1,2,4,64,1024]{4,3,2,1,0:T(8,128)(2,1)S(1)}, bf16[1,2,4,64,1024]{4,3,2,1,0:T(8,128)(2,1)}, u32[]{:S(2)}) copy-start(bf16[1,2,4,64,1024]{4,3,2,1,0:T(8,128)(2,1)} %fusion.1) | copy-start | bytes 3145732
Sparse Core Ops, SparseCore 0:
  9.5 62.2 all-gather.1

commit v2 on v1

--- a/solution.py
+++ b/solution.py
@@ -14,6 +14,7 @@
 F32 = jnp.float32
 BF16 = jnp.bfloat16
 DECAY_ROWS = 16
+CHUNKS = 4
 
 
 class Grid:
@@ -117,9 +118,7 @@
 def gather_kernel(grid, x_ref, out_ref, send_sem, recv_sem, own_sem):
     place = grid.place()
     z, y, c, x = (place[d] for d in "zycx")
-    half = x_ref.shape[1] // 2
-    first, second = pl.ds(0, half), pl.ds(half, half)
-    everything = slice(None)
+    part = x_ref.shape[1] // (2 * CHUNKS)
     grid.greet(place, ("z", "y", "c", "x"))
     own = pltpu.make_async_copy(x_ref, out_ref.at[z, y, c, x], own_sem)
     own.start()
@@ -142,27 +141,36 @@
             used += 1
         return copies
 
-    stage = push("z", x_ref, out_ref.at[z, y, c, x])
+    def start(level, t):
+        both = pl.ds(2 * t * part, 2 * part)
+        first, second = pl.ds(2 * t * part, part), pl.ds((2 * t + 1) * part, part)
+        if level == 0:
+            return push("z", x_ref.at[:, both], out_ref.at[z, y, c, x, :, both])
+        if level == 1:
+            a = out_ref.at[:, y, c, x, :, first]
+            b = out_ref.at[:, y, c, x, :, second]
+            return push("y", a, a) + push("x", b, b)
+        if level == 2:
+            a = out_ref.at[:, :, c, x, :, first]
+            b = out_ref.at[:, y, c, :, :, second]
+            return push("x", a, a) + push("y", b, b)
+        a = out_ref.at[:, :, c, :, :, both]
+        return push("c", a, a)
+
+    flying = {(0, t): start(0, t) for t in range(CHUNKS)}
     own.wait()
-    for copy in stage:
-        copy.wait()
-    a = out_ref.at[:, y, c, x, :, first]
-    b = out_ref.at[:, y, c, x, :, second]
-    stage = push("y", a, a) + push("x", b, b)
-    for copy in stage:
-        copy.wait()
-    a = out_ref.at[:, :, c, x, :, first]
-    b = out_ref.at[:, y, c, :, :, second]
-    stage = push("x", a, a) + push("y", b, b)
-    for copy in stage:
-        copy.wait()
-    a = out_ref.at[:, :, c]
-    for copy in push("c", a, a):
-        copy.wait()
+    for step in range(CHUNKS + 3):
+        for level in range(4):
+            t = step - level
+            if 0 <= t < CHUNKS:
+                for copy in flying[level, t]:
+                    copy.wait()
+                if level < 3:
+                    flying[level + 1, t] = start(level + 1, t)
 
 
 def gather(grid, array):
-    total = sum(grid.size(d) - 1 for d in "zyyxxc")
+    total = CHUNKS * sum(grid.size(d) - 1 for d in "zyyxxc")
     return pl.pallas_call(
         functools.partial(gather_kernel, grid),
         out_shape=jax.ShapeDtypeStruct(
@@ -181,20 +189,123 @@
     )(array)
 
 
+ORDERS = ("cxyz", "cyxz")
+
+
+def reduce_kernel(grid, a_ref, b_ref, out_ref, *scratch):
+    held, got, (send_sem, recv_sem, own_sem) = scratch[:2], scratch[2:10], scratch[10:]
+    terms = (a_ref, b_ref)
+    place = grid.place()
+    rows, part = held[0].shape[-2:]
+    grid.greet(place, ("z", "y", "c", "x"))
+    used = 0
+
+    def start(level, t):
+        nonlocal used
+        copies = []
+        for color in range(2):
+            dim = ORDERS[color][level]
+            n, me = grid.size(dim), place[dim]
+            for k in range(1, n):
+                to = lax.rem(me + k, n)
+                if level == 0:
+                    src = terms[color].at[to, :, :, :, :, pl.ds(t * part, part)]
+                else:
+                    before = tuple(place[d] for d in ORDERS[color][1:level])
+                    src = held[color].at[(t,) + before + (to,)]
+                copy = pltpu.make_async_remote_copy(
+                    src_ref=src,
+                    dst_ref=got[2 * level + color].at[t, k - 1],
+                    send_sem=send_sem.at[used],
+                    recv_sem=recv_sem.at[used],
+                    device_id=grid.peer(place, dim, to),
+                    device_id_type=MESH,
+                )
+                copy.start()
+                copies.append(copy)
+                used += 1
+        return copies
+
+    def add(level, t):
+        for color in range(2):
+            order = ORDERS[color]
+            here = tuple(place[d] for d in order[1 : level + 1])
+            left = [grid.size(d) for d in order[level + 1 :]]
+            peers = grid.size(order[level]) - 1
+            where = got[2 * level + color]
+
+            def block(i, _, color=color, here=here, left=left, peers=peers, where=where):
+                index, rest = [], i
+                for n in reversed(left):
+                    index.insert(0, lax.rem(rest, n))
+                    rest = rest // n
+                index = tuple(index)
+                total = held[color][(t,) + here + index].astype(F32)
+                for k in range(peers):
+                    total += where[(t, k) + index].astype(F32)
+                if level < 3:
+                    held[color][(t,) + here + index] = total.astype(BF16)
+                else:
+                    first = (color * CHUNKS + t) * part
+                    out_ref[:, first : first + part] = total
+                return 0
+
+            if left:
+                lax.fori_loop(0, math.prod(left), block, 0)
+            else:
+                block(0, 0)
+
+    flying = {(0, t): start(0, t) for t in range(CHUNKS)}
+    for t in range(CHUNKS):
+        for color in range(2):
+            own = pltpu.make_async_copy(
+                terms[color].at[place["c"], :, :, :, :, pl.ds(t * part, part)],
+                held[color].at[t],
+                own_sem.at[t, color],
+            )
+            own.start()
+            flying[0, t].append(own)
+    for step in range(CHUNKS + 3):
+        for level in range(4):
+            t = step - level
+            if 0 <= t < CHUNKS:
+                for copy in flying[level, t]:
+                    copy.wait()
+                add(level, t)
+                if level < 3:
+                    flying[level + 1, t] = start(level + 1, t)
+
+
 def reduce_scatter(grid, first, second):
-    place = grid.place()
-
-    def stage(items):
-        got = exchange(grid, items, False)
-        sums = []
-        for (array, dim), other in zip(items, got):
-            own = lax.dynamic_index_in_dim(array, place[dim], 0, keepdims=False)
-            sums.append(own.astype(F32) + jnp.sum(other.astype(F32), axis=0))
-        return sums
-
-    for dims in ("cc", "xy", "yx", "zz"):
-        first, second = stage([(first.astype(BF16), dims[0]), (second.astype(BF16), dims[1])])
-    return jnp.concatenate([first, second], axis=-1)
+    rows, cols = first.shape[-2:]
+    tile = (rows, cols // CHUNKS)
+
+    def sizes(order):
+        return tuple(grid.size(d) for d in order)
+
+    scratch = [pltpu.VMEM((CHUNKS,) + sizes(o[1:]) + tile, BF16) for o in ORDERS]
+    for level in range(4):
+        for o in ORDERS:
+            peers = grid.size(o[level]) - 1
+            scratch.append(
+                pltpu.VMEM((CHUNKS, max(peers, 1)) + sizes(o[level + 1 :]) + tile, BF16)
+            )
+    total = 2 * CHUNKS * sum(grid.size(d) - 1 for d in "cxyz")
+    return pl.pallas_call(
+        functools.partial(reduce_kernel, grid),
+        out_shape=jax.ShapeDtypeStruct((rows, 2 * cols), F32),
+        in_specs=[pl.BlockSpec(memory_space=pl.ANY)] * 2,
+        out_specs=pl.BlockSpec(memory_space=pltpu.VMEM),
+        scratch_shapes=scratch
+        + [
+            pltpu.SemaphoreType.DMA((total,)),
+            pltpu.SemaphoreType.DMA((total,)),
+            pltpu.SemaphoreType.DMA((CHUNKS, 2)),
+        ],
+        compiler_params=pltpu.CompilerParams(
+            collective_id=next(grid.ids), has_side_effects=True, vmem_limit_bytes=64000000
+        ),
+    )(first, second)
 
 
 def dot(a, b, dims, precision=None):

time: 312 us -> 262 us (0.84)
  Pallas kernels: 244 us -> 213 us
  other arithmetic: 28 us -> 9.51 us
    pallas_call x8 -> x4, Pallas kernels: 165 us -> 88.7 us  [exchange(): pl.pallas_call(functools.partial(exchange_kernel, grid, dims, keep), out_...]
    pallas_call x0 -> x1, Pallas kernels: none -> 58.8 us  [reduce_scatter(): pl.pallas_call(functools.partial(reduce_kernel, grid), out_shape=jax.Shap...]
    convert_element_type x6 -> x0, other arithmetic: 15.5 us -> none  [the longest x3 9.62 us: reduce_scatter(): second.astype(BF16)]
    pallas_call x1, Pallas kernels: 71.3 us -> 57.5 us  [gather(): pl.pallas_call(functools.partial(gather_kernel, grid), out_shape=jax.Shap...]
  transfers between devices with their start and end apart: 1 -> 1, of which waited for: 0 -> 0; matrix products, arithmetic and copies ran while one was open for 4% -> 4% of each run, Pallas kernels for 31% -> 37%
where the time goes in v2:
time: 262 us
  Pallas kernels  213 us (81%)
  matrix products  16.2 us (6%)
  between operations  13.6 us (5%)
  other arithmetic  9.51 us (4%)
  local copies, waits for them, and re-layouts  8.45 us (3%)
    pallas_call x4, Pallas kernels, exchange(): pl.pallas_call(functools.partial(exchange_kernel, grid, dims, keep), out_...  88.7 us
    pallas_call x1, Pallas kernels, reduce_scatter(): pl.pallas_call(functools.partial(reduce_kernel, grid), out_shape=jax.Shap...  58.8 us
    pallas_call x1, Pallas kernels, gather(): pl.pallas_call(functools.partial(gather_kernel, grid), out_shape=jax.Shap...  57.5 us
    dot_general x1, matrix products, on_device(): upward = jnp.dot(tokens, up, preferred_element_type=F32).astype(BF16)  6.63 us
    dot_general x2, matrix products, project(): jnp.dot(moved.reshape(-1, unit), weights, preferred_element_type=F32)  6.4 us
  transfers between devices with their start and end apart: 1, of which 0 were waited for; matrix products, arithmetic and copies ran while one was open for 4% of the time, Pallas kernels for 37%

profile of v2, /device:TPU:0, one launch (start us, length us, event | category | flops | bytes accessed | tf_op | source)
XLA Modules:
  0.0 261.8 jit_solution(5455444308881877371)
XLA Ops:
  6.5 0.0 copy-start
  6.5 0.0 all-gather.2.cloned.1.call-start
  6.5 0.7 all-gather.2.cloned.1.call-update
  7.3 1.5 copy.18.extra_ref
  8.7 4.2 %shard_map.154 = (f32[128,512]{1,0:T(8,128)}, bf16[2,128,512]{2,1,0:T(8,128)(2,1)}, bf16[2,4,128,128]{3,2,1,0:T(8,128)(2,1)}, bf16[2,4,16,128]{3,2,1,0:T(8,128)(2,1)}) custom-call(bf16[128,512]{1,0:T(8,128)(2,1)} %zf_ref.1, bf16[128,512]{1,0:T(8,128)(2,1)} %zb_ref.1, bf16[128,512]{1,0:T(8,128)(2,1)} %v_ref.1, bf16[128,512]{1,0:T(8,128)(2,1)} %q_ref.1, ...), custom_call_target="tpu_custom_call" | custom-call | tf_op jit(solution)/shard_map/pallas_call | solution.py:421
  12.9 0.8 broadcast_in_dim.8
  13.7 1.7 pad_maximum_fusion.1.refs_0_
  15.4 13.9 %shard_map.155.got_ref = bf16[16,80,128]{2,1,0:T(8,128)(2,1)} custom-call(bf16[16,80,128]{2,1,0:T(8,128)(2,1)} %pad_maximum_fusion.1.refs_0_), custom_call_target="tpu_custom_call" | custom-call | tf_op jit(solution)/shard_map/pallas_call | solution.py:102
  29.3 0.0 copy-start.1
  29.3 1.9 shard_map.156.refs_0_
  31.2 18.0 %shard_map.157 = bf16[16,64,128]{2,1,0:T(8,128)(2,1)} custom-call(bf16[16,64,128]{2,1,0:T(8,128)(2,1)} %shard_map.156.refs_0_), custom_call_target="tpu_custom_call" | custom-call | tf_op jit(solution)/shard_map/pallas_call | solution.py:102
  49.2 2.3 shard_map.158
  51.5 4.6 %shard_map.159 = bf16[2,64,512]{2,1,0:T(8,128)(2,1)} custom-call(bf16[2,64,512]{2,1,0:T(8,128)(2,1)} %bitcast.51), custom_call_target="tpu_custom_call" | custom-call | tf_op jit(solution)/shard_map/pallas_call | solution.py:102
  56.1 1.6 copy.28
  57.6 0.0 copy-done
  57.6 0.3 copy.20
  58.0 0.5 copy.21
  58.5 0.0 copy-done.1
  58.5 0.3 copy.22
  58.9 0.5 copy.23
  59.4 0.0 copy-start.2
  59.4 0.0 copy-start.3
  59.4 1.8 pad_maximum_fusion.refs_0_
  61.2 52.2 %shard_map.161 = (bf16[16,128,352]{2,1,0:T(8,128)(2,1)}, bf16[16,176,128]{2,1,0:T(8,128)(2,1)}) custom-call(bf16[16,128,352]{2,1,0:T(8,128)(2,1)} %pad_maximum_fusion.refs_0_, bf16[16,176,128]{2,1,0:T(8,128)(2,1)} %bitcast.49), custom_call_target="tpu_custom_call" | custom-call | tf_op jit(solution)/shard_map/pallas_call | solution.py:102
  113.5 0.8 constant_dynamic-slice_fusion
  114.2 0.1 maximum_reduce_fusion.1
  114.3 1.2 copy_bitcast_fusion
  115.5 0.0 copy-start.4
  115.5 0.0 all-gather.2.cloned.1.call-done
  115.6 0.0 copy-done.2
  115.6 0.0 copy-done.3
  115.6 3.2 %multiply_reduce_fusion = (f32[64]{0:T(128)S(1)}, f32[64,2048]{1,0:T(8,128)S(1)}) fusion(bf16[64,1024]{1,0:T(8,128)(2,1)S(1)} %bitcast.52, bf16[1024,2048]{1,0:T(8,128)(2,1)} %all-gather.2.cloned.1.call-done, bf16[64,2048]{1,0:T(8,128)(2,1)S(1)} %copy-done.3), kind=kOutput, calls=%fused_computation.11 | convolution fusion | flops 268959680 | bytes 5112064 | tf_op jit(solution)/shard_map/dot_general | solution.py:454
  118.8 0.0 copy-done.4
  118.8 0.8 multiply_convert_fusion.x_ref
  119.6 0.0 copy-start.5
  119.6 57.5 %shard_map.160 = bf16[4,2,2,2,64,2048]{5,4,3,2,1,0:T(8,128)(2,1)} custom-call(bf16[64,2048]{1,0:T(8,128)(2,1)} %multiply_convert_fusion.x_ref), custom_call_target="tpu_custom_call" | custom-call | tf_op jit(solution)/shard_map/pallas_call | solution.py:174
  177.1 0.0 copy-done.5
  177.1 6.6 %convolution_convert_fusion.2 = bf16[2048,352]{0,1:T(8,128)(2,1)S(1)} fusion(bf16[2048,2048]{1,0:T(8,128)(2,1)} %bitcast.41, bf16[2048,352]{1,0:T(8,128)(2,1)S(1)} %bitcast.57), kind=kOutput, calls=%fused_computation.3 | convolution fusion | flops 2953510912 | bytes 11272192 | tf_op jit(solution)/shard_map/dot_general | solution.py:460
  183.7 2.8 %multiply_add_fusion = f32[2048,352]{0,1:T(8,128)S(1)} fusion(bf16[2048,352]{0,1:T(8,128)(2,1)S(1)} %convolution_convert_fusion.2, f32[352]{0:T(512)S(1)} %get-tuple-element.19, f32[352]{0:T(512)S(1)} %get-tuple-element.18, f32[352]{0:T(512)S(1)} %get-tuple-element.17), kind=kLoop, calls=%fused_computation.2 | loop fusion | flops 5767168 | bytes 4329600 | tf_op jit(solution)/shard_map/add | solution.py:470
  186.6 0.4 fusion
  187.0 0.7 copy.24
  187.7 0.1 copy.27
  187.9 0.1 copy.25
  188.0 3.2 %convolution_convert_fusion.1 = bf16[2048,1024]{1,0:T(8,128)(2,1)} fusion(bf16[2048,176]{1,0:T(8,128)(2,1)S(1)} %bitcast.43, bf16[176,2048]{1,0:T(8,128)(2,1)S(1)} %copy_bitcast_fusion), kind=kOutput, calls=%fused_computation.1 | convolution fusion | flops 740294656 | bytes 5603328 | tf_op jit(solution)/shard_map/dot_general | solution.py:477
  191.1 3.2 %convolution_convert_fusion = bf16[2048,1024]{1,0:T(8,128)(2,1)} fusion(bf16[2048,176]{1,0:T(8,128)(2,1)S(1)} %bitcast.42, bf16[176,2048]{1,0:T(8,128)(2,1)S(1)} %copy_bitcast_fusion), kind=kOutput, calls=%fused_computation | convolution fusion | flops 740294656 | bytes 5603328 | tf_op jit(solution)/shard_map/dot_general | solution.py:477
  194.4 58.8 %shard_map.162 = f32[64,2048]{1,0:T(8,128)} custom-call(bf16[2,2,2,4,64,1024]{5,4,3,2,1,0:T(8,128)(2,1)} %bitcast.37, bf16[2,2,2,4,64,1024]{5,4,3,2,1,0:T(8,128)(2,1)} %bitcast.38), custom_call_target="tpu_custom_call" | custom-call | tf_op jit(solution)/shard_map/pallas_call | solution.py:294
  253.2 1.8 add_convert_fusion
  (1 shorter events, 0.0 us)
Async XLA Ops:
  6.5 51.1 %copy-start = (bf16[128,2816]{1,0:T(8,128)(2,1)S(1)}, bf16[128,2816]{1,0:T(8,128)(2,1)}, u32[]{:S(2)}) copy-start(bf16[128,2816]{1,0:T(8,128)(2,1)} %param.27) | copy-start | bytes 2162692
  6.5 109.0 %all-gather.2.cloned.1.call-start = ((), (), s32[]{:S(2)}) async-start(), calls=%async_computation | async-start | bytes 4456448 | tf_op jit(solution)/shard_map/all_gather | solution.py:410
  29.3 29.2 %copy-start.1 = (bf16[128,2816]{1,0:T(8,128)(2,1)S(1)}, bf16[128,2816]{1,0:T(8,128)(2,1)}, u32[]{:S(2)}) copy-start(bf16[128,2816]{1,0:T(8,128)(2,1)} %param.28) | copy-start | bytes 2162692
  59.4 56.2 %copy-start.2 = (bf16[2,8,8,512]{3,2,0,1:T(8,128)(2,1)S(1)}, bf16[2,8,8,512]{3,2,0,1:T(8,128)(2,1)}, u32[]{:S(2)}) copy-start(bf16[2,8,8,512]{3,2,0,1:T(8,128)(2,1)} %copy.28) | copy-start | bytes 393220
  59.4 56.2 %copy-start.3 = (bf16[64,2048]{1,0:T(8,128)(2,1)S(1)}, bf16[64,2048]{1,0:T(8,128)(2,1)}, u32[]{:S(2)}) copy-start(bf16[64,2048]{1,0:T(8,128)(2,1)} %param.16) | copy-start | bytes 786436
  115.5 3.2 %copy-start.4 = (f32[2048]{0:T(1024)S(1)}, f32[2048]{0:T(1024)}, u32[]{:S(2)}) copy-start(f32[2048]{0:T(1024)} %param.26) | copy-start | bytes 24580
  119.6 57.5 %copy-start.5 = (bf16[16,128,352]{2,1,0:T(8,128)(2,1)S(1)}, bf16[16,128,352]{2,1,0:T(8,128)(2,1)}, u32[]{:S(2)}) copy-start(bf16[16,128,352]{2,1,0:T(8,128)(2,1)} %get-tuple-element.15) | copy-start | bytes 4325380
Sparse Core Ops, SparseCore 0:
  9.5 62.3 all-gather.1
